TPU v7x, 32 devices: a whole 2x2x4 slice. The times are simulated.
32 devices in a mesh: sp: 8 (over z, x), tp: 4 (over y, core).
Axes of the slice: x: 2, y: 2, z: 4, core: 2. Of those that a mesh axis runs over, the one named last changes fastest.
Arguments:
- residual: bfloat16 [8192, 2048], P('sp'), may hold values from -6 to 6
- query: bfloat16 [8192, 1024], P('sp', 'tp'), may hold values from -6 to 6
- key: bfloat16 [8192, 256], P('sp', 'tp'), may hold values from -6 to 6
- value: bfloat16 [8192, 256], P('sp', 'tp'), may hold values from -6 to 6
- sink: float32 [16], P('tp'), may hold values from 3 to 9
- norm_gain: float32 [2048], replicated, may hold values from 0.1 to 1.9
- w_out: bfloat16 [1024, 2048], P('tp'), may hold values from -1.5 to 1.5
- w_gate: bfloat16 [2048, 4096], P('sp', 'tp'), may hold values from -0.125 to 0.125
- w_value: bfloat16 [2048, 4096], P('sp', 'tp'), may hold values from -0.125 to 0.125
- conv_gate: bfloat16 [3, 4096], P(None, 'tp'), may hold values from -3 to 3
- conv_value: bfloat16 [3, 4096], P(None, 'tp'), may hold values from -3 to 3
- w_down: bfloat16 [4096, 2048], P('tp', 'sp'), may hold values from -0.09375 to 0.09375
Outputs:
- layer_out: bfloat16 [8192, 2048], P(('sp', 'tp'))
All inputs are finite; a program needn't handle non-finite values.
Results may differ from a plain program's by a relative error of at most 0.015.
Values may be sent and summed in bfloat16 or wider, within the bound.
A program may use at most 128 MiB of HBM per device.

v0:
```python
import jax
import jax.numpy as jnp
from jax import lax
from jax.sharding import PartitionSpec as P

HD = 64
WINDOW = 128
THETA = 10000.0
EPS = 1e-06


def extended(block, sides, width):
    for axis, dim in sides:
        count = lax.axis_size(axis)
        forward = [(i, i + 1) for i in range(count - 1)]
        backward = [(target, source) for source, target in forward]
        low = lax.ppermute(
            lax.slice_in_dim(block, block.shape[dim] - width, None, axis=dim), axis, forward
        )
        high = lax.ppermute(lax.slice_in_dim(block, 0, width, axis=dim), axis, backward)
        block = jnp.concatenate([low, block, high], axis=dim)
    return block


def rotate(field, positions):
    count = field.shape[0]
    parts = field.astype(jnp.float32).reshape(count, -1, HD)
    inverse = 1.0 / THETA ** (jnp.arange(0, HD, 2, dtype=jnp.float32) / HD)
    angle = positions[:, None] * inverse[None, :]
    cosine = jnp.cos(angle)[:, None, :]
    sine = jnp.sin(angle)[:, None, :]
    first = parts[..., : HD // 2]
    second = parts[..., HD // 2 :]
    turned = jnp.concatenate(
        [first * cosine - second * sine, second * cosine + first * sine], axis=-1
    )
    return turned.reshape(count, -1).astype(jnp.bfloat16)


def band_attention(queries, keys, values, sinks, start, total):
    count = queries.shape[0]
    blocks = count // WINDOW
    kv_local = keys.shape[1] // HD
    group = queries.shape[1] // (kv_local * HD)
    query_blocks = queries.reshape(blocks, WINDOW, kv_local, group, HD)
    key_band = jnp.concatenate(
        [
            keys[i * WINDOW : i * WINDOW + count].reshape(blocks, WINDOW, kv_local, HD)
            for i in range(3)
        ],
        axis=1,
    )
    value_band = jnp.concatenate(
        [
            values[i * WINDOW : i * WINDOW + count].reshape(blocks, WINDOW, kv_local, HD)
            for i in range(3)
        ],
        axis=1,
    )
    scores = jnp.einsum(
        "nqkgd,njkd->nkgqj", query_blocks, key_band, preferred_element_type=jnp.float32
    ) * HD ** (-0.5)
    block_ids = jnp.arange(blocks, dtype=jnp.int32)[:, None]
    query_pos = start + block_ids * WINDOW + jnp.arange(WINDOW, dtype=jnp.int32)[None, :]
    key_pos = start - WINDOW + block_ids * WINDOW + jnp.arange(3 * WINDOW, dtype=jnp.int32)[None, :]
    valid = (
        (key_pos[:, None, :] >= 0)
        & (key_pos[:, None, :] < total)
        & (jnp.abs(query_pos[:, :, None] - key_pos[:, None, :]) <= WINDOW)
    )
    scores = jnp.where(valid[:, None, None], scores, -1e30)
    sink_col = sinks.reshape(1, kv_local, group, 1, 1)
    top = jnp.maximum(jnp.max(scores, axis=-1, keepdims=True), sink_col)
    weights = jnp.exp(scores - top)
    denom = jnp.sum(weights, axis=-1, keepdims=True) + jnp.exp(sink_col - top)
    probs = (weights / denom).astype(jnp.bfloat16)
    out = jnp.einsum("nkgqj,njkd->nqkgd", probs, value_band, preferred_element_type=jnp.float32)
    return out.reshape(count, kv_local * group * HD).astype(jnp.bfloat16)


def rmsnorm(field, gain):
    wide = field.astype(jnp.float32)
    scale = lax.rsqrt(jnp.mean(wide * wide, axis=-1, keepdims=True) + EPS)
    return (wide * scale * gain).astype(jnp.bfloat16)


def shards(
    residual,
    query,
    key,
    value,
    sink,
    norm_gain,
    w_out,
    w_gate,
    w_value,
    conv_gate,
    conv_value,
    w_down,
):
    tok_rows = query.shape[0]
    offset = lax.axis_index("sp") * tok_rows
    total = tok_rows * lax.axis_size("sp")
    share = tok_rows // lax.axis_size("tp")
    tp_index = lax.axis_index("tp")
    positions = (offset + jnp.arange(tok_rows, dtype=jnp.int32)).astype(jnp.float32)
    turned_query = rotate(query, positions)
    turned_key = rotate(key, positions)
    key_width = key.shape[1]
    band = jnp.concatenate([turned_key, value], axis=1)
    edged = extended(band, (("sp", 0),), WINDOW)
    attended = band_attention(
        turned_query, edged[:, :key_width], edged[:, key_width:], sink, offset, total
    )
    partial_value = jnp.dot(attended, w_out, preferred_element_type=jnp.float32)
    mix_full = lax.psum(partial_value.astype(jnp.bfloat16), "tp").astype(jnp.float32)
    mid_full = (residual.astype(jnp.float32) + mix_full).astype(jnp.bfloat16)
    normed = rmsnorm(mid_full, norm_gain)
    mid_rows = lax.dynamic_slice_in_dim(mid_full, tp_index * share, share, 0)
    gate_full, value_full = (
        lax.all_gather(w_gate, "sp", axis=0, tiled=True),
        lax.all_gather(w_value, "sp", axis=0, tiled=True),
    )
    gate_up = jnp.dot(normed, gate_full, preferred_element_type=jnp.float32).astype(jnp.bfloat16)
    value_up = jnp.dot(normed, value_full, preferred_element_type=jnp.float32).astype(jnp.bfloat16)
    hidden_width = gate_up.shape[1]
    stacked = jnp.concatenate([gate_up, value_up], axis=1)
    edged_up = extended(stacked, (("sp", 0),), 1).astype(jnp.float32)
    taps = jnp.concatenate([conv_gate, conv_value], axis=1).astype(jnp.float32)
    convolved = edged_up[:-2] * taps[0] + edged_up[1:-1] * taps[1] + edged_up[2:] * taps[2]
    hidden = (jax.nn.silu(convolved[:, :hidden_width]) * convolved[:, hidden_width:]).astype(
        jnp.bfloat16
    )
    terms = jnp.dot(
        hidden, lax.all_gather(w_down, "sp", axis=1, tiled=True), preferred_element_type=jnp.float32
    )
    ffn_rows = lax.psum_scatter(
        terms.astype(jnp.bfloat16), "tp", scatter_dimension=0, tiled=True
    ).astype(jnp.float32)
    return (mid_rows.astype(jnp.float32) + ffn_rows).astype(jnp.bfloat16)


def solution(mesh):
    return jax.shard_map(
        shards,
        mesh=mesh,
        in_specs=(
            P("sp", None),
            P("sp", "tp"),
            P("sp", "tp"),
            P("sp", "tp"),
            P("tp"),
            P(),
            P("tp", None),
            P("sp", "tp"),
            P("sp", "tp"),
            P(None, "tp"),
            P(None, "tp"),
            P("tp", "sp"),
        ),
        out_specs=P(("sp", "tp"), None),
        check_vma=False,
    )
```

profile of v0, /device:TPU:0, one launch (start us, length us, event | category | flops | bytes accessed | tf_op | source)
XLA Modules:
  0.0 336.9 jit_solution(1129287583386971566)
XLA Ops:
  7.4 1.0 bitcast_convert_fusion
  8.4 0.6 fusion.40
  9.0 0.8 pad_maximum_fusion.6
  9.8 4.9 %collective-permute-start = (bf16[128,128]{0,1:T(8,128)(2,1)S(1)}, bf16[128,128]{0,1:T(8,128)(2,1)S(1)}, u32[]{:S(2)}, u32[]{:S(2)}) collective-permute-start(bf16[128,128]{0,1:T(8,128)(2,1)S(1)} %get-tuple-element.19), channel_id=1, source_target_pairs={{0,4},{4,8},{8,12},{12,16},{16,20},{20,24},{24,28},{1,5},{5,9},{9,... | collective-permute-start | bytes 98312 | tf_op jit(solution)/shard_map/ppermute | solution.py:17
  14.7 1.3 collective-permute-start.1
  16.0 0.5 multiply_cosine_fusion
  16.7 1.2 copy.20
  18.3 1.2 fusion.12
  19.5 0.9 collective-permute-done.1
  20.7 1.0 fusion.6
  21.8 1.5 fusion.5
  23.5 1.9 fusion.16
  25.8 3.3 convolution_convert_fusion
  29.2 0.5 all-gather.6.cloned.1.call-update
  29.7 0.5 all-gather.4.cloned.1.call-update
  30.3 0.5 all-gather.8.cloned.1.call-update
  31.2 85.1 %all-reduce.2.cloned.1.call-done = bf16[1024,2048]{1,0:T(8,128)(2,1)} async-done(((bf16[1024,2048]{1,0:T(8,128)(2,1)}), bf16[1024,2048]{1,0:T(8,128)(2,1)}) %all-reduce.2.cloned.1.call-update) | async-done | bytes 4194320 | tf_op jit(solution)/shard_map/psum | solution.py:116
  116.2 7.4 %fusion = (f32[1024]{0:T(1024)S(1)}, bf16[1024,2048]{1,0:T(8,128)(2,1)}) fusion(bf16[1024,2048]{1,0:T(8,128)(2,1)} %all-reduce.2.cloned.1.call-done, bf16[1024,2048]{1,0:T(8,128)(2,1)} %param.12), kind=kLoop, calls=%fused_computation.2 | loop fusion | flops 14679040 | bytes 12587008 | tf_op jit(solution)/shard_map/reduce_sum | solution.py:83
  123.6 8.4 %convolution_convert_fusion.2 = bf16[1024,1024]{0,1:T(8,128)(2,1)S(1)} fusion(bf16[2048,1024]{1,0:T(8,128)(2,1)} %all-gather.6.cloned.1.call-done, bf16[1024,2048]{1,0:T(8,128)(2,1)} %get-tuple-element.6, f32[2048]{0:T(1024)S(1)} %copy-done.6, f32[1024]{0:T(1024)S(1)} %add_rsqrt_fusion), kind=kOutput, calls=%fused_computation.29 | convolution fusion | flops 4304404480 | bytes 10498048 | tf_op jit(solution)/shard_map/dot_general | solution.py:125
  132.1 46.9 %all-gather.4.cloned.1.call-done = bf16[2048,1024]{1,0:T(8,128)(2,1)} async-done(((bf16[256,1024]{1,0:T(8,128)(2,1)}), bf16[2048,1024]{1,0:T(8,128)(2,1)}) %all-gather.4.cloned.1.call-update) | async-done | bytes 4194320 | tf_op jit(solution)/shard_map/all_gather | solution.py:121
  179.0 8.4 %convolution_convert_fusion.3 = bf16[1024,1024]{0,1:T(8,128)(2,1)S(1)} fusion(bf16[2048,1024]{1,0:T(8,128)(2,1)} %all-gather.4.cloned.1.call-done, bf16[1024,2048]{1,0:T(8,128)(2,1)} %get-tuple-element.6, f32[2048]{0:T(1024)S(1)} %copy-done.6, f32[1024]{0:T(1024)S(1)} %add_rsqrt_fusion), kind=kOutput, calls=%fused_computation.30 | convolution fusion | flops 4304404480 | bytes 10498048 | tf_op jit(solution)/shard_map/dot_general | solution.py:124
  187.9 2.5 collective-permute-start.2
  190.4 1.3 collective-permute-start.3
  191.7 2.5 pad_maximum_fusion
  194.2 22.0 %collective-permute-done.2 = bf16[1,2048]{0,1:T(8,128)(2,1)S(1)} collective-permute-done((bf16[1,2048]{0,1:T(8,128)(2,1)S(1)}, bf16[1,2048]{0,1:T(8,128)(2,1)S(1)}, u32[]{:S(2)}, u32[]{:S(2)}) %collective-permute-start.2) | collective-permute-done | bytes 4128 | tf_op jit(solution)/shard_map/ppermute | solution.py:17
  216.1 9.3 %concatenate.42 = bf16[1026,2048]{0,1:T(8,128)(2,1)} concatenate(bf16[1,2048]{0,1:T(8,128)(2,1)S(1)} %collective-permute-done.2, bf16[1024,2048]{0,1:T(8,128)(2,1)} %pad_maximum_fusion, bf16[1,2048]{0,1:T(8,128)(2,1)} %collective-permute-done.3), dimensions={0} | concatenate | bytes 8404992 | tf_op jit(solution)/shard_map/concatenate | solution.py:21
  225.5 2.9 convert_element_type.108
  228.4 8.5 %fusion.3 = f32[1024,2048]{0,1:T(8,128)} fusion(f32[1026,2048]{0,1:T(8,128)S(1)} %convert_element_type.108, f32[2048]{0:T(1024)S(1)} %bitcast.117, f32[2048]{0:T(1024)S(1)} %bitcast.116, f32[2048]{0:T(1024)S(1)} %bitcast.115), kind=kLoop, calls=%fused_computation.6 | loop fusion | flops 10485760 | bytes 33579008 | tf_op jit(solution)/shard_map/add | solution.py:130
  236.9 35.2 %all-gather.8.cloned.1.call-done = bf16[1024,2048]{1,0:T(8,128)(2,1)} async-done(((bf16[1024,256]{1,0:T(8,128)(2,1)}), bf16[1024,2048]{1,0:T(8,128)(2,1)}) %all-gather.8.cloned.1.call-update) | async-done | bytes 4194320 | tf_op jit(solution)/shard_map/all_gather | solution.py:135
  272.1 11.4 %convolution_convert_fusion.1 = bf16[1024,2048]{1,0:T(8,128)(2,1)} fusion(bf16[1024,2048]{1,0:T(8,128)(2,1)} %all-gather.8.cloned.1.call-done, f32[1024,2048]{0,1:T(8,128)} %fusion.3), kind=kOutput, calls=%fused_computation.24 | convolution fusion | flops 4303355904 | bytes 16777216 | tf_op jit(solution)/shard_map/dot_general | solution.py:134
  283.5 42.9 %reduce-scatter.2.cloned.1.call-done = bf16[256,2048]{1,0:T(8,128)(2,1)} async-done(((bf16[1024,2048]{1,0:T(8,128)(2,1)}), bf16[256,2048]{1,0:T(8,128)(2,1)}) %reduce-scatter.2.cloned.1.call-update) | async-done | bytes 1048592 | tf_op jit(solution)/shard_map/reduce_scatter | solution.py:137
  326.4 2.9 add_convert_fusion.1
  (52 shorter events, 2.3 us)
Async XLA Ops:
  7.4 18.4 %copy-start = (bf16[256,2048]{1,0:T(8,128)(2,1)S(1)}, bf16[256,2048]{1,0:T(8,128)(2,1)}, u32[]{:S(2)}) copy-start(bf16[256,2048]{1,0:T(8,128)(2,1)} %param.18) | copy-start | bytes 3145732
  7.4 12.1 %copy-start.2 = (bf16[1024,64]{0,1:T(8,128)(2,1)S(1)}, bf16[1024,64]{0,1:T(8,128)(2,1)}, u32[]{:S(2)}) copy-start(bf16[1024,64]{0,1:T(8,128)(2,1)} %param.15) | copy-start | bytes 393220
  7.4 108.8 %all-reduce.2.cloned.1.call-start = ((), (), s32[]{:S(2)}) async-start(), calls=%async_computation.1 | async-start | bytes 8388608 | tf_op jit(solution)/shard_map/psum | solution.py:116
  9.8 9.7 %collective-permute-start = (bf16[128,128]{0,1:T(8,128)(2,1)S(1)}, bf16[128,128]{0,1:T(8,128)(2,1)S(1)}, u32[]{:S(2)}, u32[]{:S(2)}) collective-permute-start(bf16[128,128]{0,1:T(8,128)(2,1)S(1)} %get-tuple-element.19), channel_id=1, source_target_pairs={{0,4},{4,8},{8,12},{12,16},{16,20},{20,24},{24,28},{1,5},{5,9},{9,... | collective-permute-start | bytes 98312 | tf_op jit(solution)/shard_map/ppermute | solution.py:17
  14.7 5.8 %collective-permute-start.1 = (bf16[128,128]{0,1:T(8,128)(2,1)S(1)}, bf16[128,128]{0,1:T(8,128)(2,1)S(1)}, u32[]{:S(2)}, u32[]{:S(2)}) collective-permute-start(bf16[128,128]{0,1:T(8,128)(2,1)S(1)} %get-tuple-element.20), channel_id=1, source_target_pairs={{4,0},{8,4},{12,8},{16,12},{20,16},{24,20},{28,24},{5,1},{9,5},{13... | collective-permute-start | bytes 98312 | tf_op jit(solution)/shard_map/ppermute | solution.py:20
  20.7 1.1 copy-start.5
  29.1 2.0 copy-start.3
  29.1 2.0 copy-start.4
  29.1 94.5 %all-gather.6.cloned.1.call-start = ((), (), s32[]{:S(2)}) async-start(), calls=%async_computation.3 | async-start | bytes 4718592 | tf_op jit(solution)/shard_map/all_gather | solution.py:122
  29.7 149.3 %all-gather.4.cloned.1.call-start = ((), (), s32[]{:S(2)}) async-start(), calls=%async_computation.2 | async-start | bytes 4718592 | tf_op jit(solution)/shard_map/all_gather | solution.py:121
  30.3 241.9 %all-gather.8.cloned.1.call-start = ((), (), s32[]{:S(2)}) async-start(), calls=%async_computation.4 | async-start | bytes 4718592 | tf_op jit(solution)/shard_map/all_gather | solution.py:135
  30.9 295.6 %reduce-scatter.2.cloned.1.call-start = ((), (), s32[]{:S(2)}) async-start(), calls=%async_computation.5 | async-start | bytes 5242880 | tf_op jit(solution)/shard_map/reduce_scatter | solution.py:137
  31.1 92.5 %copy-start.6 = (f32[2048]{0:T(1024)S(1)}, f32[2048]{0:T(1024)}, u32[]{:S(2)}) copy-start(f32[2048]{0:T(1024)} %param.17) | copy-start | bytes 24580
  187.9 28.2 %collective-permute-start.2 = (bf16[1,2048]{0,1:T(8,128)(2,1)S(1)}, bf16[1,2048]{0,1:T(8,128)(2,1)S(1)}, u32[]{:S(2)}, u32[]{:S(2)}) collective-permute-start(bf16[1,2048]{0,1:T(8,128)(2,1)S(1)} %get-tuple-element.8), channel_id=1, source_target_pairs={{0,4},{4,8},{8,12},{12,16},{16,20},{20,24},{24,28},{1,5},{5,9},{9,... | collective-permute-start | bytes 12296 | tf_op jit(solution)/shard_map/ppermute | solution.py:17
  190.4 25.7 %collective-permute-start.3 = (bf16[1,2048]{0,1:T(8,128)(2,1)S(1)}, bf16[1,2048]{0,1:T(8,128)(2,1)}, u32[]{:S(2)}, u32[]{:S(2)}) collective-permute-start(bf16[1,2048]{0,1:T(8,128)(2,1)S(1)} %get-tuple-element.7), channel_id=1, source_target_pairs={{4,0},{8,4},{12,8},{16,12},{20,16},{24,20},{28,24},{5,1},{9,5},{13... | collective-permute-start | bytes 12296 | tf_op jit(solution)/shard_map/ppermute | solution.py:20
  272.1 57.2 %copy-start.1 = (bf16[256,2048]{1,0:T(8,128)(2,1)S(1)}, bf16[256,2048]{1,0:T(8,128)(2,1)}, u32[]{:S(2)}) copy-start(bf16[256,2048]{1,0:T(8,128)(2,1)} %param.18) | copy-start | bytes 3145732
Sparse Core Ops, SparseCore 0:
  29.2 86.9 all-reduce.1
  283.7 42.7 reduce-scatter.1
Sparse Core Ops, SparseCore 1:
  31.7 74.0 all-gather.5
  107.8 71.1 all-gather.3
  180.9 91.2 all-gather.7
where the time goes:
time: 338 us; the launch traced here: 337 us
  waiting for transfers between devices  235 us (70%)
  matrix products  34.4 us (10%)
  other arithmetic  31.1 us (9%)
  between operations  15.4 us (5%)
  local copies, waits for them, and re-layouts  11.2 us (3%)
  starting transfers between devices  10.3 us (3%)
    psum x1, waiting for transfers between devices, shards(): lax.psum(partial_value.astype(jnp.bfloat16), 'tp').astype(jnp.float32)  85.1 us
    all_gather x1, waiting for transfers between devices, shards(): lax.all_gather(w_gate, 'sp', axis=0, tiled=True)  46.9 us
    reduce_scatter x1, waiting for transfers between devices, shards(): lax.psum_scatter(terms.astype(jnp.bfloat16), 'tp', scatter_dimension=0, t...  42.9 us
    all_gather x1, waiting for transfers between devices, shards(): lax.all_gather(w_down, 'sp', axis=1, tiled=True)  35.2 us
    ppermute x2, waiting for transfers between devices, extended(): lax.ppermute(lax.slice_in_dim(block, block.shape[dim] - width, None, axis...  22 us
    dot_general x1, matrix products, shards(): jnp.dot(hidden, lax.all_gather(w_down, 'sp', axis=1, tiled=True), preferr...  11.4 us
    concatenate x1, local copies, waits for them, and re-layouts, extended(): block = jnp.concatenate([low, block, high], axis=dim)  9.35 us
    add x1, other arithmetic, shards(): edged_up[:-2] * taps[0] + edged_up[1:-1] * taps[1] + edged_up[2:] * taps[2]  8.49 us
  transfers between devices with their start and end apart: 9, of which 6 were waited for; matrix products, arithmetic and copies ran while one was open for 15% of the time, Pallas kernels for 0%

commit v1 on v0

--- a/solution.py
+++ b/solution.py
@@ -7,6 +7,12 @@
 WINDOW = 128
 THETA = 10000.0
 EPS = 1e-06
+
+
+def add_all(block, mesh_axis):
+    terms = lax.all_gather(block, mesh_axis, axis=0, tiled=False)
+    total = terms.sum(axis=0)
+    return total
 
 
 def extended(block, sides, width):
@@ -113,7 +119,7 @@
         turned_query, edged[:, :key_width], edged[:, key_width:], sink, offset, total
     )
     partial_value = jnp.dot(attended, w_out, preferred_element_type=jnp.float32)
-    mix_full = lax.psum(partial_value.astype(jnp.bfloat16), "tp").astype(jnp.float32)
+    mix_full = add_all(partial_value.astype(jnp.bfloat16), "tp").astype(jnp.float32)
     mid_full = (residual.astype(jnp.float32) + mix_full).astype(jnp.bfloat16)
     normed = rmsnorm(mid_full, norm_gain)
     mid_rows = lax.dynamic_slice_in_dim(mid_full, tp_index * share, share, 0)

time: 338 us -> 442 us (1.31)
  waiting for transfers between devices: 235 us -> 329 us
  other arithmetic: 31.1 us -> 43.1 us
    all_gather x0 -> x1, waiting for transfers between devices: none -> 105 us  [add_all(): terms = lax.all_gather(block, mesh_axis, axis=0, tiled=False)]
    psum x1 -> x0, waiting for transfers between devices: 85.1 us -> none  [shards(): lax.psum(partial_value.astype(jnp.bfloat16), 'tp').astype(jnp.float32)]
    all_gather x1, waiting for transfers between devices: 0.01 us -> 55.3 us  [shards(): lax.all_gather(w_value, 'sp', axis=0, tiled=True)]
    all_gather x1, waiting for transfers between devices: 46.9 us -> 65.1 us  [shards(): lax.all_gather(w_gate, 'sp', axis=0, tiled=True)]
    reduce_sum x0 -> x1, other arithmetic: none -> 12.2 us  [add_all(): total = terms.sum(axis=0)]
  transfers between devices with their start and end apart: 9 -> 9, of which waited for: 6 -> 7; matrix products, arithmetic and copies ran while one was open for 15% -> 14% of each run, Pallas kernels for 0% -> 0%
where the time goes in v1:
time: 442 us; the launch traced here: 441 us
  waiting for transfers between devices  329 us (74%)
  other arithmetic  43.1 us (10%)
  matrix products  34.6 us (8%)
  between operations  13.5 us (3%)
  local copies, waits for them, and re-layouts  11.2 us (3%)
  starting transfers between devices  10.1 us (2%)
    all_gather x1, waiting for transfers between devices, add_all(): terms = lax.all_gather(block, mesh_axis, axis=0, tiled=False)  105 us
    all_gather x1, waiting for transfers between devices, shards(): lax.all_gather(w_gate, 'sp', axis=0, tiled=True)  65.1 us
    all_gather x1, waiting for transfers between devices, shards(): lax.all_gather(w_value, 'sp', axis=0, tiled=True)  55.3 us
    reduce_scatter x1, waiting for transfers between devices, shards(): lax.psum_scatter(terms.astype(jnp.bfloat16), 'tp', scatter_dimension=0, t...  42.9 us
    all_gather x1, waiting for transfers between devices, shards(): lax.all_gather(w_down, 'sp', axis=1, tiled=True)  35.5 us
    ppermute x2, waiting for transfers between devices, extended(): lax.ppermute(lax.slice_in_dim(block, block.shape[dim] - width, None, axis...  21.9 us
    reduce_sum x1, other arithmetic, add_all(): total = terms.sum(axis=0)  12.2 us
    dot_general x1, matrix products, shards(): jnp.dot(hidden, lax.all_gather(w_down, 'sp', axis=1, tiled=True), preferr...  11.4 us
  transfers between devices with their start and end apart: 9, of which 7 were waited for; matrix products, arithmetic and copies ran while one was open for 14% of the time, Pallas kernels for 0%

profile of v1, /device:TPU:0, one launch (start us, length us, event | category | flops | bytes accessed | tf_op | source)
XLA Modules:
  0.0 441.4 jit_solution(7684666861331852566)
XLA Ops:
  6.6 1.0 bitcast_convert_fusion
  7.6 0.6 fusion.40
  8.2 0.7 pad_maximum_fusion.6
  9.0 4.9 %collective-permute-start = (bf16[128,128]{0,1:T(8,128)(2,1)S(1)}, bf16[128,128]{0,1:T(8,128)(2,1)S(1)}, u32[]{:S(2)}, u32[]{:S(2)}) collective-permute-start(bf16[128,128]{0,1:T(8,128)(2,1)S(1)} %get-tuple-element.19), channel_id=1, source_target_pairs={{0,4},{4,8},{8,12},{12,16},{16,20},{20,24},{24,28},{1,5},{5,9},{9,... | collective-permute-start | bytes 98312 | tf_op jit(solution)/shard_map/ppermute | solution.py:23
  13.8 1.3 collective-permute-start.1
  15.8 1.2 copy.20
  17.4 1.2 fusion.12
  18.7 0.9 collective-permute-done.1
  19.8 1.0 fusion.6
  21.0 1.5 fusion.5
  22.7 1.9 fusion.16
  25.0 3.2 convolution_convert_fusion
  28.3 0.7 all-gather.8.cloned.1.call-update
  29.0 0.7 all-gather.6.cloned.1.call-update
  30.4 105.4 %all-gather.12.cloned.1.call-done = bf16[4096,2048]{1,0:T(8,128)(2,1)} async-done(((bf16[1024,2048]{1,0:T(8,128)(2,1)}), bf16[4096,2048]{1,0:T(8,128)(2,1)}) %all-gather.12.cloned.1.call-update) | async-done | bytes 16777232 | tf_op jit(solution)/shard_map/all_gather | solution.py:13
  135.8 12.2 %reduce_sum.31 = bf16[1024,2048]{1,0:T(8,128)(2,1)} reduce(bf16[4,1024,2048]{2,1,0:T(8,128)(2,1)} %bitcast.107, bf16[]{:T(256)} %constant.44.clone.1), dimensions={0}, to_apply=%region_2.3 | reduce | flops 6291456 | bytes 20971522 | tf_op jit(solution)/shard_map/reduce_sum | solution.py:14
  148.0 7.4 %fusion = (f32[1024]{0:T(1024)S(1)}, bf16[1024,2048]{1,0:T(8,128)(2,1)}) fusion(bf16[1024,2048]{1,0:T(8,128)(2,1)} %reduce_sum.31, bf16[1024,2048]{1,0:T(8,128)(2,1)} %param.12), kind=kLoop, calls=%fused_computation.2 | loop fusion | flops 14679040 | bytes 12587008 | tf_op jit(solution)/shard_map/reduce_sum | solution.py:89
  155.4 55.3 %all-gather.8.cloned.1.call-done = bf16[2048,1024]{1,0:T(8,128)(2,1)} async-done(((bf16[256,1024]{1,0:T(8,128)(2,1)}), bf16[2048,1024]{1,0:T(8,128)(2,1)}) %all-gather.8.cloned.1.call-update) | async-done | bytes 4194320 | tf_op jit(solution)/shard_map/all_gather | solution.py:128
  210.7 8.4 %convolution_convert_fusion.2 = bf16[1024,1024]{0,1:T(8,128)(2,1)S(1)} fusion(bf16[2048,1024]{1,0:T(8,128)(2,1)} %all-gather.8.cloned.1.call-done, bf16[1024,2048]{1,0:T(8,128)(2,1)} %get-tuple-element.6, f32[2048]{0:T(1024)S(1)} %copy-done.6, f32[1024]{0:T(1024)S(1)} %add_rsqrt_fusion), kind=kOutput, calls=%fused_computation.29 | convolution fusion | flops 4304404480 | bytes 10498048 | tf_op jit(solution)/shard_map/dot_general | solution.py:131
  219.1 65.1 %all-gather.6.cloned.1.call-done = bf16[2048,1024]{1,0:T(8,128)(2,1)} async-done(((bf16[256,1024]{1,0:T(8,128)(2,1)}), bf16[2048,1024]{1,0:T(8,128)(2,1)}) %all-gather.6.cloned.1.call-update) | async-done | bytes 4194320 | tf_op jit(solution)/shard_map/all_gather | solution.py:127
  284.2 8.6 %convolution_convert_fusion.3 = bf16[1024,1024]{0,1:T(8,128)(2,1)S(1)} fusion(bf16[2048,1024]{1,0:T(8,128)(2,1)} %all-gather.6.cloned.1.call-done, bf16[1024,2048]{1,0:T(8,128)(2,1)} %get-tuple-element.6, f32[2048]{0:T(1024)S(1)} %copy-done.6, f32[1024]{0:T(1024)S(1)} %add_rsqrt_fusion), kind=kOutput, calls=%fused_computation.30 | convolution fusion | flops 4304404480 | bytes 10498048 | tf_op jit(solution)/shard_map/dot_general | solution.py:130
  293.1 2.5 collective-permute-start.2
  295.6 1.3 collective-permute-start.3
  296.9 2.6 pad_maximum_fusion
  299.5 21.9 %collective-permute-done.2 = bf16[1,2048]{0,1:T(8,128)(2,1)S(1)} collective-permute-done((bf16[1,2048]{0,1:T(8,128)(2,1)S(1)}, bf16[1,2048]{0,1:T(8,128)(2,1)S(1)}, u32[]{:S(2)}, u32[]{:S(2)}) %collective-permute-start.2) | collective-permute-done | bytes 4128 | tf_op jit(solution)/shard_map/ppermute | solution.py:23
  321.4 9.3 %concatenate.42 = bf16[1026,2048]{0,1:T(8,128)(2,1)} concatenate(bf16[1,2048]{0,1:T(8,128)(2,1)S(1)} %collective-permute-done.2, bf16[1024,2048]{0,1:T(8,128)(2,1)} %pad_maximum_fusion, bf16[1,2048]{0,1:T(8,128)(2,1)} %collective-permute-done.3), dimensions={0} | concatenate | bytes 8404992 | tf_op jit(solution)/shard_map/concatenate | solution.py:27
  330.7 2.9 convert_element_type.110
  333.7 8.5 %fusion.3 = f32[1024,2048]{0,1:T(8,128)} fusion(f32[1026,2048]{0,1:T(8,128)S(1)} %convert_element_type.110, f32[2048]{0:T(1024)S(1)} %bitcast.119, f32[2048]{0:T(1024)S(1)} %bitcast.118, f32[2048]{0:T(1024)S(1)} %bitcast.117), kind=kLoop, calls=%fused_computation.6 | loop fusion | flops 10485760 | bytes 33579008 | tf_op jit(solution)/shard_map/add | solution.py:136
  342.2 35.5 %all-gather.10.cloned.1.call-done = bf16[1024,2048]{1,0:T(8,128)(2,1)} async-done(((bf16[1024,256]{1,0:T(8,128)(2,1)}), bf16[1024,2048]{1,0:T(8,128)(2,1)}) %all-gather.10.cloned.1.call-update) | async-done | bytes 4194320 | tf_op jit(solution)/shard_map/all_gather | solution.py:141
  377.6 11.4 %convolution_convert_fusion.1 = bf16[1024,2048]{1,0:T(8,128)(2,1)} fusion(bf16[1024,2048]{1,0:T(8,128)(2,1)} %all-gather.10.cloned.1.call-done, f32[1024,2048]{0,1:T(8,128)} %fusion.3), kind=kOutput, calls=%fused_computation.24 | convolution fusion | flops 4303355904 | bytes 16777216 | tf_op jit(solution)/shard_map/dot_general | solution.py:140
  389.1 42.9 %reduce-scatter.2.cloned.1.call-done = bf16[256,2048]{1,0:T(8,128)(2,1)} async-done(((bf16[1024,2048]{1,0:T(8,128)(2,1)}), bf16[256,2048]{1,0:T(8,128)(2,1)}) %reduce-scatter.2.cloned.1.call-update) | async-done | bytes 1048592 | tf_op jit(solution)/shard_map/reduce_scatter | solution.py:143
  432.0 2.9 add_convert_fusion.1
  (53 shorter events, 2.9 us)
Async XLA Ops:
  6.5 18.4 %copy-start = (bf16[256,2048]{1,0:T(8,128)(2,1)S(1)}, bf16[256,2048]{1,0:T(8,128)(2,1)}, u32[]{:S(2)}) copy-start(bf16[256,2048]{1,0:T(8,128)(2,1)} %param.18) | copy-start | bytes 3145732
  6.5 12.1 %copy-start.2 = (bf16[1024,64]{0,1:T(8,128)(2,1)S(1)}, bf16[1024,64]{0,1:T(8,128)(2,1)}, u32[]{:S(2)}) copy-start(bf16[1024,64]{0,1:T(8,128)(2,1)} %param.15) | copy-start | bytes 393220
  6.5 129.2 %all-gather.12.cloned.1.call-start = ((), (), s32[]{:S(2)}) async-start(), calls=%async_computation.5 | async-start | bytes 20971520 | tf_op jit(solution)/shard_map/all_gather | solution.py:13
  9.0 9.7 %collective-permute-start = (bf16[128,128]{0,1:T(8,128)(2,1)S(1)}, bf16[128,128]{0,1:T(8,128)(2,1)S(1)}, u32[]{:S(2)}, u32[]{:S(2)}) collective-permute-start(bf16[128,128]{0,1:T(8,128)(2,1)S(1)} %get-tuple-element.19), channel_id=1, source_target_pairs={{0,4},{4,8},{8,12},{12,16},{16,20},{20,24},{24,28},{1,5},{5,9},{9,... | collective-permute-start | bytes 98312 | tf_op jit(solution)/shard_map/ppermute | solution.py:23
  13.8 5.8 %collective-permute-start.1 = (bf16[128,128]{0,1:T(8,128)(2,1)S(1)}, bf16[128,128]{0,1:T(8,128)(2,1)S(1)}, u32[]{:S(2)}, u32[]{:S(2)}) collective-permute-start(bf16[128,128]{0,1:T(8,128)(2,1)S(1)} %get-tuple-element.20), channel_id=1, source_target_pairs={{4,0},{8,4},{12,8},{16,12},{20,16},{24,20},{28,24},{5,1},{9,5},{13... | collective-permute-start | bytes 98312 | tf_op jit(solution)/shard_map/ppermute | solution.py:26
  19.8 1.1 copy-start.5
  28.2 2.1 copy-start.3
  28.2 2.1 copy-start.4
  28.2 182.5 %all-gather.8.cloned.1.call-start = ((), (), s32[]{:S(2)}) async-start(), calls=%async_computation.2 | async-start | bytes 4718592 | tf_op jit(solution)/shard_map/all_gather | solution.py:128
  29.0 255.2 %all-gather.6.cloned.1.call-start = ((), (), s32[]{:S(2)}) async-start(), calls=%async_computation.1 | async-start | bytes 4718592 | tf_op jit(solution)/shard_map/all_gather | solution.py:127
  29.7 347.9 %all-gather.10.cloned.1.call-start = ((), (), s32[]{:S(2)}) async-start(), calls=%async_computation.3 | async-start | bytes 4718592 | tf_op jit(solution)/shard_map/all_gather | solution.py:141
  30.3 401.7 %reduce-scatter.2.cloned.1.call-start = ((), (), s32[]{:S(2)}) async-start(), calls=%async_computation.4 | async-start | bytes 5242880 | tf_op jit(solution)/shard_map/reduce_scatter | solution.py:143
  148.0 62.7 %copy-start.6 = (f32[2048]{0:T(1024)S(1)}, f32[2048]{0:T(1024)}, u32[]{:S(2)}) copy-start(f32[2048]{0:T(1024)} %param.17) | copy-start | bytes 24580
  293.1 28.2 %collective-permute-start.2 = (bf16[1,2048]{0,1:T(8,128)(2,1)S(1)}, bf16[1,2048]{0,1:T(8,128)(2,1)S(1)}, u32[]{:S(2)}, u32[]{:S(2)}) collective-permute-start(bf16[1,2048]{0,1:T(8,128)(2,1)S(1)} %get-tuple-element.8), channel_id=1, source_target_pairs={{0,4},{4,8},{8,12},{12,16},{16,20},{20,24},{24,28},{1,5},{5,9},{9,... | collective-permute-start | bytes 12296 | tf_op jit(solution)/shard_map/ppermute | solution.py:23
  295.6 25.7 %collective-permute-start.3 = (bf16[1,2048]{0,1:T(8,128)(2,1)S(1)}, bf16[1,2048]{0,1:T(8,128)(2,1)}, u32[]{:S(2)}, u32[]{:S(2)}) collective-permute-start(bf16[1,2048]{0,1:T(8,128)(2,1)S(1)} %get-tuple-element.7), channel_id=1, source_target_pairs={{4,0},{8,4},{12,8},{16,12},{20,16},{24,20},{28,24},{5,1},{9,5},{13... | collective-permute-start | bytes 12296 | tf_op jit(solution)/shard_map/ppermute | solution.py:26
  377.6 57.2 %copy-start.1 = (bf16[256,2048]{1,0:T(8,128)(2,1)S(1)}, bf16[256,2048]{1,0:T(8,128)(2,1)}, u32[]{:S(2)}) copy-start(bf16[256,2048]{1,0:T(8,128)(2,1)} %param.18) | copy-start | bytes 3145732
Sparse Core Ops, SparseCore 0:
  28.4 107.3 all-gather.11
  137.9 72.7 all-gather.7
  212.8 71.3 all-gather.5
  286.1 91.5 all-gather.9
  389.2 42.7 reduce-scatter.1
